TPU v7x, 32 devices: a whole 2x2x4 slice. The times are simulated.
32 devices in a mesh: ep: 8 (over z, y), tp: 4 (over x, core).
Axes of the slice: x: 2, y: 2, z: 4, core: 2. Of those that a mesh axis runs over, the one named last changes fastest.
Arguments:
- queries: bfloat16 [4096, 1024], P('ep', 'tp'), may hold values from -6 to 6
- key_rows: bfloat16 [4096, 512], P('ep', 'tp'), may hold values from -6 to 6
- value_rows: bfloat16 [4096, 512], P('ep', 'tp'), may hold values from -6 to 6
- forget_logit: float32 [8, 4096], P('tp', 'ep'), may hold values from -1 to 17
- out_weight: bfloat16 [1024, 2048], P('tp'), may hold values from -0.1875 to 0.1875
- out_gain: float32 [2048], replicated, may hold values from 0.1 to 1.9
- moe_input: bfloat16 [4096, 2048], P('ep'), may hold values from -6 to 6
- moe_gain: float32 [2048], replicated, may hold values from 0.1 to 1.9
- router_group: bfloat16 [2048, 4], replicated, may hold values from -2 to 2
- router_expert: bfloat16 [2048, 8], replicated, may hold values from -0.125 to 0.125
- route_group: int32 [4096], P('ep'), may hold values from 0 to 3
- route_pick: int32 [4096, 2], P('ep'), may hold values from 0 to 1, as said below
- expert_gate: bfloat16 [8, 2048, 1024], P('ep', None, 'tp'), may hold values from -0.125 to 0.125
- expert_up: bfloat16 [8, 2048, 1024], P('ep', None, 'tp'), may hold values from -0.125 to 0.125
- expert_down: bfloat16 [8, 1024, 2048], P('ep', 'tp'), may hold values from -42 to 42
Outputs:
- mixer_out: bfloat16 [4096, 2048], P(('ep', 'tp'))
- moe_out: bfloat16 [4096, 2048], P(('ep', 'tp'))
Inputs may be any that keep to these rules, and one draw needn't show every extreme that they name: `route_pick`: the two entries of a row differ.
All inputs are finite; a program needn't handle non-finite values.
Results may differ from a plain program's by a relative error of at most 0.013.
Values may be sent and summed in bfloat16 or wider, within the bound.
A program may use at most 128 MiB of HBM per device.

v0:
```python
import math
import jax
import jax.numpy as jnp
from jax import lax
from jax.sharding import PartitionSpec as P

DH = 128
GROUPS = 4


def rms_scale(row_block, scale_gain):
    values = row_block.astype(jnp.float32)
    return (
        values * lax.rsqrt(jnp.mean(values * values, axis=-1, keepdims=True) + 1e-06) * scale_gain
    )


def slot_ranks(chosen, block_rows, experts):
    expert_ids = jnp.arange(experts, dtype=jnp.int32)
    matches = chosen[:, :, None] == expert_ids
    usage = jnp.any(matches, axis=1).astype(jnp.int32)
    grouped = usage.reshape(-1, block_rows, experts)
    before = (jnp.cumsum(grouped, axis=1) - grouped).reshape(-1, experts)
    return jnp.sum(jnp.where(matches, before[:, None, :], 0), axis=2)


def expert_hidden(arrived, gate_part, up_part):
    flat = arrived.reshape(-1, arrived.shape[-1])
    gated = jnp.dot(flat, gate_part, preferred_element_type=jnp.float32)
    lifted = jnp.dot(flat, up_part, preferred_element_type=jnp.float32)
    hidden = (jax.nn.silu(gated) * lifted).astype(jnp.bfloat16)
    return hidden.reshape(arrived.shape[:-1] + (gate_part.shape[1],))


def body(
    queries,
    key_rows,
    value_rows,
    forget_logit,
    out_weight,
    out_gain,
    moe_input,
    moe_gain,
    router_group,
    router_expert,
    route_group,
    route_pick,
    expert_gate,
    expert_up,
    expert_down,
):
    tp_count = lax.axis_size("tp")
    ep_count = lax.axis_size("ep")
    tp_index = lax.axis_index("tp")
    ep_index = lax.axis_index("ep")
    rows_group = queries.shape[0]
    query_heads = forget_logit.shape[0]
    key_heads = key_rows.shape[1] // DH
    ratio = query_heads // key_heads
    own_start = ep_index * rows_group
    own_pos = own_start + jnp.arange(rows_group, dtype=jnp.int32)
    local_cum = jnp.cumsum(jax.nn.log_sigmoid(forget_logit), axis=1)
    every_cum = lax.all_gather(local_cum, "ep", axis=1, tiled=True).reshape(
        query_heads, ep_count, rows_group
    )
    shard_totals = every_cum[:, :, -1]
    offsets = jnp.cumsum(shard_totals, axis=1) - shard_totals
    cum_gate = (every_cum + offsets[:, :, None]).reshape(query_heads, ep_count * rows_group)
    own_cum = lax.dynamic_slice_in_dim(cum_gate, own_start, rows_group, 1).reshape(
        key_heads, ratio, rows_group, 1
    )
    query_stack = (
        queries.reshape(rows_group, key_heads, ratio, DH)
        .transpose(1, 2, 0, 3)
        .reshape(key_heads, ratio * rows_group, DH)
    )

    def attend_block(current, keys_block, values_block, start):
        piece_rows = keys_block.shape[0]

        def compute(state):
            row_top, row_total, weighted = state
            key_stack = keys_block.reshape(piece_rows, key_heads, DH).transpose(1, 0, 2)
            value_stack = values_block.reshape(piece_rows, key_heads, DH).transpose(1, 0, 2)
            scores = jnp.einsum(
                "gqd,gkd->gqk", query_stack, key_stack, preferred_element_type=jnp.float32
            ) / math.sqrt(DH)
            key_cum = lax.dynamic_slice_in_dim(cum_gate, start, piece_rows, 1).reshape(
                key_heads, ratio, 1, piece_rows
            )
            logits = scores.reshape(key_heads, ratio, rows_group, piece_rows) + own_cum - key_cum
            visible = (start + jnp.arange(piece_rows, dtype=jnp.int32))[None, :] <= own_pos[:, None]
            logits = jnp.where(visible, logits, -1e30)
            new_top = jnp.maximum(row_top, jnp.max(logits, axis=3))
            expo = jnp.where(visible, jnp.exp(logits - new_top[..., None]), 0.0)
            rescale = jnp.exp(row_top - new_top)
            row_total = row_total * rescale + jnp.sum(expo, axis=3)
            product = jnp.einsum(
                "gqk,gkd->gqd",
                expo.reshape(key_heads, ratio * rows_group, piece_rows).astype(jnp.bfloat16),
                value_stack,
                preferred_element_type=jnp.float32,
            )
            weighted = weighted * rescale.reshape(key_heads, ratio * rows_group, 1) + product
            return (new_top, row_total, weighted)

        return lax.cond(start < own_start + rows_group, compute, lambda state: state, current)

    initial = (
        jnp.full((key_heads, ratio, rows_group), -1e30, jnp.float32),
        jnp.zeros((key_heads, ratio, rows_group), jnp.float32),
        jnp.zeros((key_heads, ratio * rows_group, DH), jnp.float32),
    )
    current = initial
    keys_piece = lax.all_gather(key_rows, "ep", axis=0, tiled=True)
    values_piece = lax.all_gather(value_rows, "ep", axis=0, tiled=True)
    piece_rows = keys_piece.shape[0]
    blocks = piece_rows // rows_group

    def advance(state, inputs):
        keys_block, values_block, block_index = inputs
        return (attend_block(state, keys_block, values_block, block_index * rows_group), None)

    current, _ = lax.scan(
        advance,
        current,
        (
            keys_piece.reshape(blocks, rows_group, -1),
            values_piece.reshape(blocks, rows_group, -1),
            jnp.arange(blocks, dtype=jnp.int32),
        ),
    )
    row_top, row_total, weighted = current
    attended = (weighted / row_total.reshape(key_heads, ratio * rows_group, 1)).astype(jnp.bfloat16)
    attended = (
        attended.reshape(key_heads, ratio, rows_group, DH)
        .transpose(2, 0, 1, 3)
        .reshape(rows_group, query_heads * DH)
    )
    group_rows = moe_input.shape[0]
    own_rows = group_rows // tp_count
    width_model = moe_input.shape[1]
    experts = expert_gate.shape[0] * ep_count
    per_group = experts // GROUPS
    capacity = tp_count * own_rows // experts
    own_first = tp_index * own_rows
    chosen_all = route_group[:, None] * per_group + route_pick
    rank_all = slot_ranks(chosen_all, own_rows, experts)
    chosen = lax.dynamic_slice_in_dim(chosen_all, own_first, own_rows, 0)
    ranks = lax.dynamic_slice_in_dim(rank_all, own_first, own_rows, 0)
    is_kept = ranks < capacity
    own_group = lax.dynamic_slice_in_dim(route_group, own_first, own_rows, 0)
    normed = rms_scale(
        lax.dynamic_slice_in_dim(moe_input, own_first, own_rows, 0), moe_gain
    ).astype(jnp.bfloat16)
    target = jnp.where(is_kept, chosen * capacity + ranks, experts * capacity)
    sources = jnp.broadcast_to(jnp.arange(own_rows, dtype=jnp.int32)[:, None], target.shape)
    slot_table = (
        jnp.full((experts * capacity,), own_rows, jnp.int32)
        .at[target.reshape(-1)]
        .set(sources.reshape(-1), mode="drop")
    )
    padded = jnp.concatenate([normed, jnp.zeros((1, width_model), jnp.bfloat16)], axis=0)
    outgoing = padded[slot_table].reshape(experts, capacity, width_model)
    arrived = lax.all_to_all(outgoing, "ep", split_axis=0, concat_axis=0, tiled=True)
    hidden_arrived = lax.all_gather(arrived[None], "tp", axis=0, tiled=True)
    hidden = expert_hidden(hidden_arrived, expert_gate[0], expert_up[0])
    hidden_rows = hidden.reshape(-1, hidden.shape[-1])
    mixer_term = jnp.dot(attended, out_weight, preferred_element_type=jnp.float32)
    expert_term = jnp.dot(hidden_rows, expert_down[0], preferred_element_type=jnp.float32)
    mixer_summed, expert_summed = (
        lax.psum_scatter(
            mixer_term.astype(jnp.bfloat16), "tp", scatter_dimension=0, tiled=True
        ).astype(jnp.float32),
        lax.psum_scatter(
            expert_term.astype(jnp.bfloat16), "tp", scatter_dimension=0, tiled=True
        ).astype(jnp.float32),
    )
    mixer_out = rms_scale(mixer_summed, out_gain).astype(jnp.bfloat16)
    group_logits = jnp.dot(normed, router_group, preferred_element_type=jnp.float32)
    expert_logits = jnp.dot(normed, router_expert, preferred_element_type=jnp.float32)
    group_top = jnp.max(group_logits, axis=1, keepdims=True)
    group_exp = jnp.exp(group_logits - group_top)
    group_hit = jnp.arange(GROUPS, dtype=jnp.int32)[None, :] == own_group[:, None]
    group_share = jnp.sum(jnp.where(group_hit, group_exp, 0.0), axis=1) / jnp.sum(group_exp, axis=1)
    expert_hit = jnp.arange(experts, dtype=jnp.int32)[None, None, :] == chosen[:, :, None]
    picked_logits = jnp.sum(jnp.where(expert_hit, expert_logits[:, None, :], 0.0), axis=2)
    shares = group_share[:, None] * jax.nn.sigmoid(picked_logits - picked_logits[:, ::-1])
    results = expert_summed.astype(jnp.bfloat16).reshape(ep_count, capacity, width_model)
    returned = lax.all_to_all(results, "ep", split_axis=0, concat_axis=0, tiled=True).reshape(
        experts * capacity, width_model
    )
    slot_index = jnp.where(is_kept, chosen * capacity + ranks, 0)
    picked = returned[slot_index]
    moe_out = jnp.sum(
        jnp.where(is_kept, shares, 0.0)[:, :, None] * picked.astype(jnp.float32), axis=1
    )
    return (mixer_out, moe_out.astype(jnp.bfloat16))


def solution(mesh):
    in_specs = (
        P("ep", "tp"),
        P("ep", "tp"),
        P("ep", "tp"),
        P("tp", "ep"),
        P("tp", None),
        P(),
        P("ep", None),
        P(),
        P(),
        P(),
        P("ep"),
        P("ep", None),
        P("ep", None, "tp"),
        P("ep", None, "tp"),
        P("ep", "tp", None),
    )
    out_specs = (P(("ep", "tp"), None), P(("ep", "tp"), None))
    return jax.shard_map(body, mesh=mesh, in_specs=in_specs, out_specs=out_specs, check_vma=False)
```

profile of v0, /device:TPU:0, one launch (start us, length us, event | category | flops | bytes accessed | tf_op | source)
XLA Modules:
  0.0 390.1 jit_solution(8046871968145064070)
XLA Ops:
  7.2 0.8 broadcast_multiply_fusion
  8.0 0.8 dynamic_slice.47
  8.8 0.7 broadcast_add_fusion.1
  9.5 1.2 fusion.22
  10.7 1.3 fusion.24
  12.0 1.0 fusion.40
  12.9 0.2 fusion.41
  13.2 0.1 copy.78
  13.4 0.3 reduce_window_sum.42
  13.9 0.1 copy.81
  14.0 0.1 reshape.280
  14.2 0.1 reshape.307
  14.3 1.4 scatter_custom_fusion
  15.8 3.3 gather_fusion
  19.1 55.6 %all_to_all.10 = bf16[8,64,2048]{2,1,0:T(8,128)(2,1)} all-to-all(bf16[8,64,2048]{2,1,0:T(8,128)(2,1)} %bitcast.87), channel_id=1, replica_groups=mesh['ep'=8,'tp'=4] {'ep'}, dimensions={0} | all-to-all | bytes 4194304 | tf_op jit(solution)/shard_map/all_to_all | solution.py:165
  74.8 0.7 all-gather.7.cloned.1.call-update
  75.6 0.7 all-gather.5.cloned.1.call-update
  76.3 55.9 %all-gather.9.cloned.1.call-done = bf16[32,64,2048]{2,1,0:T(8,128)(2,1)} async-done(((bf16[8,64,2048]{2,1,0:T(8,128)(2,1)}), bf16[32,64,2048]{2,1,0:T(8,128)(2,1)}) %all-gather.9.cloned.1.call-update) | async-done | bytes 8388624 | tf_op jit(solution)/shard_map/all_gather | solution.py:166
  132.2 7.2 %fusion.28 = f32[2048,256]{1,0:T(8,128)} fusion(bf16[2048,2048]{1,0:T(8,128)(2,1)} %bitcast.104, bf16[1,2048,256]{2,1,0:T(8,128)(2,1)S(1)} %copy-done.7), kind=kOutput, calls=%fused_computation.46 | convolution fusion | flops 2147483648 | bytes 11534336 | tf_op jit(solution)/shard_map/dot_general | solution.py:29
  139.4 13.2 %convolution_convert_fusion = bf16[2048,2048]{1,0:T(8,128)(2,1)} fusion(bf16[2048,2048]{1,0:T(8,128)(2,1)} %bitcast.105, f32[2048,256]{1,0:T(8,128)} %fusion.28, bf16[1,256,2048]{2,1,0:T(8,128)(2,1)S(1)} %copy-done, bf16[1,2048,256]{2,1,0:T(8,128)(2,1)S(1)} %copy-done.8), kind=kOutput, calls=%fused_computation.28 | convolution fusion | flops 4302307328 | bytes 20971520 | tf_op jit(solution)/shard_map/dot_general | solution.py:170
  152.6 0.6 copy-done.6
  153.3 0.6 reduce-window.6
  153.9 0.2 slice_reduce_fusion
  154.1 0.2 reduce-window.9
  154.3 0.1 copy.83
  154.5 51.7 %all_gather.13 = f32[2,4096]{0,1:T(8,128)S(1)} all-gather(f32[2,512]{0,1:T(8,128)S(1)} %bitcast.92), channel_id=1, replica_groups=mesh['ep'=8,'tp'=4] {'ep'}, dimensions={1}, use_global_device_ids=true | all-gather | bytes 36864 | tf_op jit(solution)/shard_map/all_gather | solution.py:63
  206.3 0.2 reduce_window_sum.41
  206.6 1.4 bitcast_add_fusion
  208.0 1.0 dynamic-slice_bitcast_fusion
  209.3 23.2 %all-gather.5.cloned.1.call-done = bf16[4096,128]{1,0:T(8,128)(2,1)} async-done(((bf16[512,128]{1,0:T(8,128)(2,1)}), bf16[4096,128]{1,0:T(8,128)(2,1)}) %all-gather.5.cloned.1.call-update) | async-done | bytes 1048592 | tf_op jit(solution)/shard_map/all_gather | solution.py:115
  232.5 0.8 broadcast_in_dim.103
  233.4 20.4 %while.17 = (s32[]{:T(128)}, f32[1,2,512]{2,1,0:T(2,128)S(1)}, f32[1,2,512]{2,1,0:T(2,128)S(1)}, f32[1,1024,128]{2,1,0:T(8,128)}, s32[8]{0:T(128)S(1)}, /*index=...) while((s32[]{:T(128)}, f32[1,2,512]{2,1,0:T(2,128)S(1)}, ...), condition=%wide.region_8.9_spmd.clone, body=%wide.region_3.8_spmd.clone.sunk | while | flops 274731008 | bytes 24245672 | solution.py:124
  233.4 0.6 dynamic_slice.81
  234.6 10.0 %conditional.3 = ((f32[1,2,512]{2,1,0:T(2,128)S(1)}, f32[1,2,512]{2,1,0:T(2,128)S(1)}, f32[1,1024,128]{2,1,0:T(8,128)})) conditional(s32[]{:T(128)} %convert_element_type.103, (f32[1,2,512]{2,1,0:T(2,128)S(1)}, f32[1,2,512]{2,1,0:T(2,128)S(1)}, f32[1,1024,128]{2,1,0:T(8,128)}) %tuple.59, (s32[]{:T(128)}, s32[]{:T(128)}, ...), branch_computations={%region_4.4_spmd, %region_5.7_spmd} | conditional | flops 274731008 | bytes 24243334 | solution.py:107
  234.6 0.2 broadcast_compare_fusion
  234.9 0.1 broadcast_in_dim.47
  235.0 1.4 copy.69
  236.4 1.0 constant_dynamic-slice_fusion
  237.4 0.7 sub.59
  238.1 0.5 copy.87
  238.6 0.7 copy-done.1
  239.3 1.6 fusion.39
  240.9 3.2 fusion.5
  244.1 0.5 fusion.4
  244.6 0.6 dynamic_slice.81
  246.0 0.6 dynamic_slice.81
  247.3 0.6 dynamic_slice.81
  248.6 0.6 dynamic_slice.81
  249.9 0.6 dynamic_slice.81
  251.2 0.6 dynamic_slice.81
  252.4 0.6 dynamic_slice.81
  253.7 1.2 divide_convert_fusion
  255.0 0.1 copy.77
  255.2 3.3 convolution_convert_fusion.1
  258.4 46.7 %reduce-scatter.5.cloned.1.call-done = bf16[512,2048]{1,0:T(8,128)(2,1)} async-done(((bf16[2048,2048]{1,0:T(8,128)(2,1)}), bf16[512,2048]{1,0:T(8,128)(2,1)}) %reduce-scatter.5.cloned.1.call-update) | async-done | bytes 2097168 | tf_op jit(solution)/shard_map/reduce_scatter | solution.py:175
  305.1 23.7 %all-to-all-start.1 = ((bf16[8,64,2048]{2,1,0:T(8,128)(2,1)}), bf16[8,64,2048]{2,1,0:T(8,128)(2,1)S(1)}, u32[]{:S(2)}, u32[]{:S(2)}) async-start(bf16[8,64,2048]{2,1,0:T(8,128)(2,1)} %bitcast.88), calls=%async_computation.3 | async-start | bytes 4194304 | tf_op jit(solution)/shard_map/all_to_all | solution.py:190
  328.9 0.1 reshape.297
  329.1 26.1 %reduce-scatter.3.cloned.1.call-done = bf16[128,2048]{1,0:T(8,128)(2,1)} async-done(((bf16[512,2048]{1,0:T(8,128)(2,1)}), bf16[128,2048]{1,0:T(8,128)(2,1)}) %reduce-scatter.3.cloned.1.call-update) | async-done | bytes 524304 | tf_op jit(solution)/shard_map/reduce_scatter | solution.py:172
  355.2 1.2 fusion.19
  356.5 2.0 fusion.21
  358.5 16.4 %all-to-all-done.1 = bf16[8,64,2048]{2,1,0:T(8,128)(2,1)S(1)} async-done(((bf16[8,64,2048]{2,1,0:T(8,128)(2,1)}), bf16[8,64,2048]{2,1,0:T(8,128)(2,1)S(1)}, u32[]{:S(2)}, u32[]{:S(2)}) %all-to-all-start.1) | async-done | bytes 2097184 | tf_op jit(solution)/shard_map/all_to_all | solution.py:190
  374.9 2.3 gather_fusion.1
  377.2 2.4 reshape.316
  379.6 3.9 %multiply_reduce_fusion = bf16[128,2048]{1,0:T(8,128)(2,1)} fusion(f32[128,2,2048]{2,1,0:T(2,128)S(1)} %reshape.316, f32[128,2]{1,0:T(8,128)S(1)} %copy.80), kind=kLoop, calls=%fused_computation.33 | loop fusion | flops 786432 | bytes 2622464 | tf_op jit(solution)/shard_map/reduce_sum | solution.py:195
  (84 shorter events, 1.6 us)
Async XLA Ops:
  7.2 132.2 %copy-start = (bf16[1,256,2048]{2,1,0:T(8,128)(2,1)S(1)}, bf16[1,256,2048]{2,1,0:T(8,128)(2,1)}, u32[]{:S(2)}) copy-start(bf16[1,256,2048]{2,1,0:T(8,128)(2,1)} %param.33) | copy-start | bytes 3145732
  7.2 5.8 %copy-start.4 = (bf16[2048,8]{0,1:T(8,128)(2,1)S(1)}, bf16[2048,8]{0,1:T(8,128)(2,1)}, u32[]{:S(2)}) copy-start(bf16[2048,8]{0,1:T(8,128)(2,1)} %param.28) | copy-start | bytes 98308
  7.2 125.0 %all-gather.9.cloned.1.call-start = ((), (), s32[]{:S(2)}) async-start(), calls=%async_computation.8 | async-start | bytes 10485760 | tf_op jit(solution)/shard_map/all_gather | solution.py:166
  74.7 57.5 %copy-start.7 = (bf16[1,2048,256]{2,1,0:T(8,128)(2,1)S(1)}, bf16[1,2048,256]{2,1,0:T(8,128)(2,1)}, u32[]{:S(2)}) copy-start(bf16[1,2048,256]{2,1,0:T(8,128)(2,1)} %param.31) | copy-start | bytes 3145732
  74.8 134.5 %all-gather.7.cloned.1.call-start = ((), (), s32[]{:S(2)}) async-start(), calls=%async_computation.5 | async-start | bytes 1179648 | tf_op jit(solution)/shard_map/all_gather | solution.py:116
  75.5 157.0 %all-gather.5.cloned.1.call-start = ((), (), s32[]{:S(2)}) async-start(), calls=%async_computation.4 | async-start | bytes 1179648 | tf_op jit(solution)/shard_map/all_gather | solution.py:115
  76.2 228.9 %reduce-scatter.5.cloned.1.call-start = ((), (), s32[]{:S(2)}) async-start(), calls=%async_computation.7 | async-start | bytes 10485760 | tf_op jit(solution)/shard_map/reduce_scatter | solution.py:175
  132.2 7.2 %copy-start.8 = (bf16[1,2048,256]{2,1,0:T(8,128)(2,1)S(1)}, bf16[1,2048,256]{2,1,0:T(8,128)(2,1)}, u32[]{:S(2)}) copy-start(bf16[1,2048,256]{2,1,0:T(8,128)(2,1)} %param.32) | copy-start | bytes 3145732
  152.6 0.7 copy-start.6
  152.6 202.6 %reduce-scatter.3.cloned.1.call-start = ((), (), s32[]{:S(2)}) async-start(), calls=%async_computation.6 | async-start | bytes 2621440 | tf_op jit(solution)/shard_map/reduce_scatter | solution.py:172
  206.6 2.5 copy-start.3
  238.1 1.2 copy-start.1
  240.9 3.2 copy-start.2
  305.1 51.4 %copy-start.5 = (f32[2048]{0:T(1024)S(1)}, f32[2048]{0:T(1024)}, u32[]{:S(2)}) copy-start(f32[2048]{0:T(1024)} %param.24) | copy-start | bytes 24580
  305.1 69.8 %all-to-all-start.1 = ((bf16[8,64,2048]{2,1,0:T(8,128)(2,1)}), bf16[8,64,2048]{2,1,0:T(8,128)(2,1)S(1)}, u32[]{:S(2)}, u32[]{:S(2)}) async-start(bf16[8,64,2048]{2,1,0:T(8,128)(2,1)} %bitcast.88), calls=%async_computation.3 | async-start | bytes 4194304 | tf_op jit(solution)/shard_map/all_to_all | solution.py:190
Sparse Core Ops, SparseCore 0:
  74.9 57.2 all-gather.8
  134.3 52.7 all-gather.6
  189.2 43.2 all-gather.4
  234.9 70.0 reduce-scatter.4
  307.5 47.7 reduce-scatter.2
where the time goes:
time: 392 us; the launch traced here: 390 us
  waiting for transfers between devices  170 us (43%)
  blocking collectives  107 us (27%)
  matrix products  29.6 us (8%)
  starting transfers between devices  23.9 us (6%)
  local copies, waits for them, and re-layouts  23.7 us (6%)
  other arithmetic  16.1 us (4%)
  between operations  14 us (4%)
  loops' own time  5.77 us (1%)
    all_gather x1, waiting for transfers between devices, body(): hidden_arrived = lax.all_gather(arrived[None], 'tp', axis=0, tiled=True)  55.9 us
    all_to_all x1, blocking collectives, body(): lax.all_to_all(outgoing, 'ep', split_axis=0, concat_axis=0, tiled=True)  55.6 us
    all_gather x1, blocking collectives, body(): lax.all_gather(local_cum, 'ep', axis=1, tiled=True)  51.7 us
    reduce_scatter x1, waiting for transfers between devices, body(): lax.psum_scatter(expert_term.astype(jnp.bfloat16), 'tp', scatter_dimensio...  46.7 us
    reduce_scatter x1, waiting for transfers between devices, body(): lax.psum_scatter(mixer_term.astype(jnp.bfloat16), 'tp', scatter_dimension...  26.1 us
    all_to_all x1, starting transfers between devices, body(): lax.all_to_all(results, 'ep', split_axis=0, concat_axis=0, tiled=True)  23.7 us
    all_gather x1, waiting for transfers between devices, body(): keys_piece = lax.all_gather(key_rows, 'ep', axis=0, tiled=True)  23.2 us
    all_to_all x1, waiting for transfers between devices, body(): lax.all_to_all(results, 'ep', split_axis=0, concat_axis=0, tiled=True)  16.4 us
  transfers between devices with their start and end apart: 6, of which 5 were waited for; matrix products, arithmetic and copies ran while one was open for 12% of the time, Pallas kernels for 0%

commit v1 on v0

--- a/solution.py
+++ b/solution.py
@@ -60,7 +60,7 @@
     own_start = ep_index * rows_group
     own_pos = own_start + jnp.arange(rows_group, dtype=jnp.int32)
     local_cum = jnp.cumsum(jax.nn.log_sigmoid(forget_logit), axis=1)
-    every_cum = lax.all_gather(local_cum, "ep", axis=1, tiled=True).reshape(
+    every_cum = jnp.concatenate(lax.all_gather(local_cum, "ep"), axis=1).reshape(
         query_heads, ep_count, rows_group
     )
     shard_totals = every_cum[:, :, -1]

time: 392 us -> 375 us (0.957)
  blocking collectives: 107 us -> 86.5 us
  waiting for transfers between devices: 170 us -> 175 us
    all_gather x1, blocking collectives: 51.7 us -> 30.9 us  [body(): lax.all_gather(local_cum, 'ep')]
    all_gather x1, waiting for transfers between devices: 23.2 us -> 28.1 us  [body(): keys_piece = lax.all_gather(key_rows, 'ep', axis=0, tiled=True)]
  transfers between devices with their start and end apart: 6 -> 6, of which waited for: 5 -> 5; matrix products, arithmetic and copies ran while one was open for 12% -> 13% of each run, Pallas kernels for 0% -> 0%
where the time goes in v1:
time: 375 us; the launch traced here: 373 us
  waiting for transfers between devices  175 us (47%)
  blocking collectives  86.5 us (23%)
  matrix products  29.6 us (8%)
  local copies, waits for them, and re-layouts  24.4 us (7%)
  starting transfers between devices  23.9 us (6%)
  other arithmetic  14.6 us (4%)
  between operations  14 us (4%)
  loops' own time  5.76 us (2%)
    all_gather x1, waiting for transfers between devices, body(): hidden_arrived = lax.all_gather(arrived[None], 'tp', axis=0, tiled=True)  55.9 us
    all_to_all x1, blocking collectives, body(): lax.all_to_all(outgoing, 'ep', split_axis=0, concat_axis=0, tiled=True)  55.6 us
    reduce_scatter x1, waiting for transfers between devices, body(): lax.psum_scatter(expert_term.astype(jnp.bfloat16), 'tp', scatter_dimensio...  46.7 us
    all_gather x1, blocking collectives, body(): lax.all_gather(local_cum, 'ep')  30.9 us
    all_gather x1, waiting for transfers between devices, body(): keys_piece = lax.all_gather(key_rows, 'ep', axis=0, tiled=True)  28.1 us
    reduce_scatter x1, waiting for transfers between devices, body(): lax.psum_scatter(mixer_term.astype(jnp.bfloat16), 'tp', scatter_dimension...  26.1 us
    all_to_all x1, starting transfers between devices, body(): lax.all_to_all(results, 'ep', split_axis=0, concat_axis=0, tiled=True)  23.7 us
    all_to_all x1, waiting for transfers between devices, body(): lax.all_to_all(results, 'ep', split_axis=0, concat_axis=0, tiled=True)  16.4 us
  transfers between devices with their start and end apart: 6, of which 5 were waited for; matrix products, arithmetic and copies ran while one was open for 13% of the time, Pallas kernels for 0%

profile of v1, /device:TPU:0, one launch (start us, length us, event | category | flops | bytes accessed | tf_op | source)
XLA Modules:
  0.0 373.3 jit_solution(567576422183413724)
XLA Ops:
  7.2 0.8 broadcast_multiply_fusion
  8.0 0.8 dynamic_slice.47
  8.8 0.7 broadcast_add_fusion.2
  9.5 1.2 fusion.22
  10.7 1.3 fusion.24
  12.0 1.0 fusion.41
  12.9 0.2 fusion.42
  13.2 0.1 copy.87
  13.4 0.3 reduce_window_sum.48
  13.7 0.1 copy.88
  13.9 0.1 copy.90
  14.0 0.1 reshape.300
  14.2 0.1 reshape.327
  14.3 1.4 scatter_custom_fusion
  15.8 3.3 gather_fusion
  19.1 55.6 %all_to_all.10 = bf16[8,64,2048]{2,1,0:T(8,128)(2,1)} all-to-all(bf16[8,64,2048]{2,1,0:T(8,128)(2,1)} %bitcast.84), channel_id=1, replica_groups=mesh['ep'=8,'tp'=4] {'ep'}, dimensions={0} | all-to-all | bytes 4194304 | tf_op jit(solution)/shard_map/all_to_all | solution.py:165
  74.8 0.7 all-gather.7.cloned.1.call-update
  75.6 0.7 all-gather.5.cloned.1.call-update
  76.3 55.9 %all-gather.9.cloned.1.call-done = bf16[32,64,2048]{2,1,0:T(8,128)(2,1)} async-done(((bf16[8,64,2048]{2,1,0:T(8,128)(2,1)}), bf16[32,64,2048]{2,1,0:T(8,128)(2,1)}) %all-gather.9.cloned.1.call-update) | async-done | bytes 8388624 | tf_op jit(solution)/shard_map/all_gather | solution.py:166
  132.2 7.2 %fusion.28 = f32[2048,256]{1,0:T(8,128)} fusion(bf16[2048,2048]{1,0:T(8,128)(2,1)} %bitcast.104, bf16[1,2048,256]{2,1,0:T(8,128)(2,1)S(1)} %copy-done.7), kind=kOutput, calls=%fused_computation.46 | convolution fusion | flops 2147483648 | bytes 11534336 | tf_op jit(solution)/shard_map/dot_general | solution.py:29
  139.4 13.2 %convolution_convert_fusion = bf16[2048,2048]{1,0:T(8,128)(2,1)} fusion(bf16[2048,2048]{1,0:T(8,128)(2,1)} %bitcast.105, f32[2048,256]{1,0:T(8,128)} %fusion.28, bf16[1,256,2048]{2,1,0:T(8,128)(2,1)S(1)} %copy-done, bf16[1,2048,256]{2,1,0:T(8,128)(2,1)S(1)} %copy-done.8), kind=kOutput, calls=%fused_computation.28 | convolution fusion | flops 4302307328 | bytes 20971520 | tf_op jit(solution)/shard_map/dot_general | solution.py:170
  152.7 0.6 copy-done.6
  153.3 0.6 reduce-window.6
  153.9 0.2 slice_reduce_fusion
  154.1 0.2 reduce-window.9
  154.3 30.9 %all_gather.14 = f32[8,2,512]{2,1,0:T(2,128)S(1)} all-gather(f32[1,2,512]{2,1,0:T(2,128)S(1)} %reduce_window_sum.46), channel_id=1, replica_groups=mesh['ep'=8,'tp'=4] {'ep'}, dimensions={0}, use_global_device_ids=true | all-gather | bytes 36864 | tf_op jit(solution)/shard_map/all_gather | solution.py:63
  185.6 2.0 copy.85
  187.7 28.1 %all-gather.5.cloned.1.call-done = bf16[4096,128]{1,0:T(8,128)(2,1)} async-done(((bf16[512,128]{1,0:T(8,128)(2,1)}), bf16[4096,128]{1,0:T(8,128)(2,1)}) %all-gather.5.cloned.1.call-update) | async-done | bytes 1048592 | tf_op jit(solution)/shard_map/all_gather | solution.py:115
  215.7 0.8 broadcast_in_dim.103
  216.6 20.4 %while.17 = (s32[]{:T(128)}, f32[1,2,512]{2,1,0:T(2,128)S(1)}, f32[1,2,512]{2,1,0:T(2,128)S(1)}, f32[1,1024,128]{2,1,0:T(8,128)}, s32[8]{0:T(128)S(1)}, /*index=...) while((s32[]{:T(128)}, f32[1,2,512]{2,1,0:T(2,128)S(1)}, ...), condition=%wide.region_8.9_spmd.clone, body=%wide.region_3.8_spmd.clone.sunk | while | flops 274731008 | bytes 24245672 | solution.py:124
  216.6 0.6 dynamic_slice.81
  217.8 10.0 %conditional.3 = ((f32[1,2,512]{2,1,0:T(2,128)S(1)}, f32[1,2,512]{2,1,0:T(2,128)S(1)}, f32[1,1024,128]{2,1,0:T(8,128)})) conditional(s32[]{:T(128)} %convert_element_type.103, (f32[1,2,512]{2,1,0:T(2,128)S(1)}, f32[1,2,512]{2,1,0:T(2,128)S(1)}, f32[1,1024,128]{2,1,0:T(8,128)}) %tuple.60, (s32[]{:T(128)}, s32[]{:T(128)}, ...), branch_computations={%region_4.4_spmd, %region_5.7_spmd} | conditional | flops 274731008 | bytes 24243334 | solution.py:107
  217.9 0.2 broadcast_compare_fusion
  218.1 0.1 broadcast_in_dim.47
  218.2 1.4 copy.79
  219.6 1.0 constant_dynamic-slice_fusion
  220.6 0.7 sub.59
  221.3 0.5 copy.92
  221.8 0.7 copy-done.1
  222.5 1.6 fusion.40
  224.2 3.2 fusion.5
  227.3 0.5 fusion.4
  227.9 0.6 dynamic_slice.81
  229.2 0.6 dynamic_slice.81
  230.5 0.6 dynamic_slice.81
  231.8 0.6 dynamic_slice.81
  233.1 0.6 dynamic_slice.81
  234.4 0.6 dynamic_slice.81
  235.7 0.6 dynamic_slice.81
  237.0 1.2 divide_convert_fusion
  238.2 0.1 copy.86
  238.4 3.3 convolution_convert_fusion.1
  241.7 46.7 %reduce-scatter.5.cloned.1.call-done = bf16[512,2048]{1,0:T(8,128)(2,1)} async-done(((bf16[2048,2048]{1,0:T(8,128)(2,1)}), bf16[512,2048]{1,0:T(8,128)(2,1)}) %reduce-scatter.5.cloned.1.call-update) | async-done | bytes 2097168 | tf_op jit(solution)/shard_map/reduce_scatter | solution.py:175
  288.3 23.7 %all-to-all-start.1 = ((bf16[8,64,2048]{2,1,0:T(8,128)(2,1)}), bf16[8,64,2048]{2,1,0:T(8,128)(2,1)S(1)}, u32[]{:S(2)}, u32[]{:S(2)}) async-start(bf16[8,64,2048]{2,1,0:T(8,128)(2,1)} %bitcast.85), calls=%async_computation.3 | async-start | bytes 4194304 | tf_op jit(solution)/shard_map/all_to_all | solution.py:190
  312.0 0.1 copy.91
  312.1 0.1 reshape.317
  312.2 0.1 copy.89
  312.4 26.1 %reduce-scatter.3.cloned.1.call-done = bf16[128,2048]{1,0:T(8,128)(2,1)} async-done(((bf16[512,2048]{1,0:T(8,128)(2,1)}), bf16[128,2048]{1,0:T(8,128)(2,1)}) %reduce-scatter.3.cloned.1.call-update) | async-done | bytes 524304 | tf_op jit(solution)/shard_map/reduce_scatter | solution.py:172
  338.4 1.2 fusion.19
  339.7 2.0 fusion.21
  341.7 16.4 %all-to-all-done.1 = bf16[8,64,2048]{2,1,0:T(8,128)(2,1)S(1)} async-done(((bf16[8,64,2048]{2,1,0:T(8,128)(2,1)}), bf16[8,64,2048]{2,1,0:T(8,128)(2,1)S(1)}, u32[]{:S(2)}, u32[]{:S(2)}) %all-to-all-start.1) | async-done | bytes 2097184 | tf_op jit(solution)/shard_map/all_to_all | solution.py:190
  358.1 2.3 gather_fusion.1
  360.4 2.4 reshape.336
  362.8 3.9 %multiply_reduce_fusion = bf16[128,2048]{1,0:T(8,128)(2,1)} fusion(f32[128,2,2048]{2,1,0:T(2,128)S(1)} %reshape.336, f32[128,2]{1,0:T(8,128)S(1)} %copy.89), kind=kLoop, calls=%fused_computation.32 | loop fusion | flops 786432 | bytes 2622464 | tf_op jit(solution)/shard_map/reduce_sum | solution.py:195
  (83 shorter events, 1.4 us)
Async XLA Ops:
  7.2 132.2 %copy-start = (bf16[1,256,2048]{2,1,0:T(8,128)(2,1)S(1)}, bf16[1,256,2048]{2,1,0:T(8,128)(2,1)}, u32[]{:S(2)}) copy-start(bf16[1,256,2048]{2,1,0:T(8,128)(2,1)} %param.33) | copy-start | bytes 3145732
  7.2 5.8 %copy-start.4 = (bf16[2048,8]{0,1:T(8,128)(2,1)S(1)}, bf16[2048,8]{0,1:T(8,128)(2,1)}, u32[]{:S(2)}) copy-start(bf16[2048,8]{0,1:T(8,128)(2,1)} %param.28) | copy-start | bytes 98308
  7.2 125.0 %all-gather.9.cloned.1.call-start = ((), (), s32[]{:S(2)}) async-start(), calls=%async_computation.8 | async-start | bytes 10485760 | tf_op jit(solution)/shard_map/all_gather | solution.py:166
  74.7 57.5 %copy-start.7 = (bf16[1,2048,256]{2,1,0:T(8,128)(2,1)S(1)}, bf16[1,2048,256]{2,1,0:T(8,128)(2,1)}, u32[]{:S(2)}) copy-start(bf16[1,2048,256]{2,1,0:T(8,128)(2,1)} %param.31) | copy-start | bytes 3145732
  74.8 112.9 %all-gather.7.cloned.1.call-start = ((), (), s32[]{:S(2)}) async-start(), calls=%async_computation.5 | async-start | bytes 1179648 | tf_op jit(solution)/shard_map/all_gather | solution.py:116
  75.5 140.2 %all-gather.5.cloned.1.call-start = ((), (), s32[]{:S(2)}) async-start(), calls=%async_computation.4 | async-start | bytes 1179648 | tf_op jit(solution)/shard_map/all_gather | solution.py:115
  76.2 212.1 %reduce-scatter.5.cloned.1.call-start = ((), (), s32[]{:S(2)}) async-start(), calls=%async_computation.7 | async-start | bytes 10485760 | tf_op jit(solution)/shard_map/reduce_scatter | solution.py:175
  132.2 7.2 %copy-start.8 = (bf16[1,2048,256]{2,1,0:T(8,128)(2,1)S(1)}, bf16[1,2048,256]{2,1,0:T(8,128)(2,1)}, u32[]{:S(2)}) copy-start(bf16[1,2048,256]{2,1,0:T(8,128)(2,1)} %param.32) | copy-start | bytes 3145732
  152.6 0.7 copy-start.6
  152.6 34.9 %copy-start.3 = (bf16[512,256]{1,0:T(8,128)(2,1)S(1)}, bf16[512,256]{1,0:T(8,128)(2,1)}, u32[]{:S(2)}) copy-start(bf16[512,256]{1,0:T(8,128)(2,1)} %param.19) | copy-start | bytes 786436
  152.6 185.8 %reduce-scatter.3.cloned.1.call-start = ((), (), s32[]{:S(2)}) async-start(), calls=%async_computation.6 | async-start | bytes 2621440 | tf_op jit(solution)/shard_map/reduce_scatter | solution.py:172
  221.3 1.2 copy-start.1
  224.1 3.2 copy-start.2
  288.3 51.3 %copy-start.5 = (f32[2048]{0:T(1024)S(1)}, f32[2048]{0:T(1024)}, u32[]{:S(2)}) copy-start(f32[2048]{0:T(1024)} %param.24) | copy-start | bytes 24580
  288.3 69.8 %all-to-all-start.1 = ((bf16[8,64,2048]{2,1,0:T(8,128)(2,1)}), bf16[8,64,2048]{2,1,0:T(8,128)(2,1)S(1)}, u32[]{:S(2)}, u32[]{:S(2)}) async-start(bf16[8,64,2048]{2,1,0:T(8,128)(2,1)} %bitcast.85), calls=%async_computation.3 | async-start | bytes 4194304 | tf_op jit(solution)/shard_map/all_to_all | solution.py:190
Sparse Core Ops, SparseCore 0:
  74.9 57.2 all-gather.8
  134.3 40.3 all-gather.6
  176.9 38.8 all-gather.4
  218.2 70.0 reduce-scatter.4
  290.7 47.6 reduce-scatter.2
